TPU v7x, 32 devices: a whole 2x2x4 slice. The times are simulated.
32 devices in a mesh: grp: 2 (over y), fs: 4 (over z), tp: 4 (over x, core).
Axes of the slice: x: 2, y: 2, z: 4, core: 2. Of those that a mesh axis runs over, the one named last changes fastest.
Arguments:
- tokens: bfloat16 [8192, 2048], P(('grp', 'fs'), 'tp'), parts along dimension 0, may hold values from -6 to 6
- norm1_gain: float32 [2048], replicated, may hold values from 0.1 to 1.9
- weight_u: float32 [2048, 1024], P('fs', 'tp'), may hold values from -0.125 to 0.125
- weight_v: float32 [2048, 1024], P('fs', 'tp'), may hold values from -0.125 to 0.125
- scale_u: float32 [1024], P('tp'), may hold values from 0.5 to 2
- scale_v: float32 [1024], P('tp'), may hold values from 0.05 to 4.5
- mix_gain: float32 [1024], P('tp'), may hold values from 0.1 to 1.9
- spatial_weight: float32 [4, 128, 128], replicated, may hold values from -0.5 to 0.5
- spatial_bias: float32 [4, 128], replicated, may hold values from 0.5 to 1.5
- weight_out: float32 [1024, 2048], P('tp', 'fs'), may hold values from -0.1875 to 0.1875
- scale_out: float32 [2048], P('fs'), may hold values from 0.5 to 2
- norm2_gain: float32 [2048], replicated, may hold values from 0.1 to 1.9
- weight_up: float32 [2048, 8192], P('fs', 'tp'), may hold values from -0.125 to 0.125
- scale_up: float32 [8192], P('tp'), may hold values from 0.5 to 2
- weight_down: float32 [8192, 2048], P('tp', 'fs'), may hold values from -0.0625 to 0.0625
- scale_down: float32 [2048], P('fs'), may hold values from 0.5 to 2
Outputs:
- result: bfloat16 [8192, 2048], P(('grp', 'fs'), 'tp'), parts along dimension 0
There are 2 independent parts, one for each index of `grp`. A program takes and returns all parts, laid end to end along the dimension named above; an argument that names none is the same for every part. Nothing has to cross between parts.
All inputs are finite; a program needn't handle non-finite values.
Results may differ from a plain program's by a relative error of at most 0.023.
Values may be sent and summed in bfloat16 or wider, within the bound.
A program may use at most 128 MiB of HBM per device.

v0:
```python
import jax
import jax.numpy as jnp
from jax import lax
from jax.sharding import PartitionSpec as P

GM_W = 1024
GROUPS = 4
BLOCK = 128


def per_device(
    tokens,
    norm1_gain,
    weight_u,
    weight_v,
    scale_u,
    scale_v,
    mix_gain,
    spatial_weight,
    spatial_bias,
    weight_out,
    scale_out,
    norm2_gain,
    weight_up,
    scale_up,
    weight_down,
    scale_down,
):
    feature_count = norm1_gain.shape[0]
    out_scales, down_scales = (
        lax.all_gather(scale_out, "fs", axis=0, tiled=True),
        lax.all_gather(scale_down, "fs", axis=0, tiled=True),
    )
    full_u, full_v = (
        lax.all_gather(weight_u.astype(jnp.bfloat16), "fs", axis=0, tiled=True),
        lax.all_gather(weight_v.astype(jnp.bfloat16), "fs", axis=0, tiled=True),
    )
    widened_in = tokens.astype(jnp.float32)
    squares_in = lax.psum(jnp.sum(widened_in * widened_in, axis=1), "tp")
    inverse_in = lax.rsqrt(squares_in / feature_count + 1e-06)[:, None]
    gain_piece = norm1_gain
    normed_piece = (
        lax.all_gather(tokens, "tp", axis=1, tiled=True).astype(jnp.float32)
        * inverse_in
        * gain_piece
    ).astype(jnp.bfloat16)
    pre_u = jnp.dot(normed_piece, full_u, preferred_element_type=jnp.float32)
    pre_v = jnp.dot(normed_piece, full_v, preferred_element_type=jnp.float32)
    gate_u = jax.nn.gelu(pre_u * scale_u)
    act_v = jax.nn.gelu(pre_v * scale_v)
    local_width = act_v.shape[1]
    row_sums, row_squares = lax.psum((jnp.sum(act_v, axis=1), jnp.sum(act_v * act_v, axis=1)), "tp")
    row_mean = (row_sums / GM_W)[:, None]
    square = (row_squares / GM_W)[:, None]
    v_norm = (
        (act_v - row_mean) * lax.rsqrt(square - row_mean * row_mean + 1e-06) * mix_gain
    ).astype(jnp.bfloat16)
    group_index = lax.axis_index("tp") * local_width // (GM_W // GROUPS)
    lower_mask = jnp.tril(jnp.ones((BLOCK, BLOCK), jnp.float32))
    spatial_mask = (
        lax.dynamic_index_in_dim(spatial_weight, group_index, 0, keepdims=False) * lower_mask
    ).astype(jnp.bfloat16)
    block_bias = lax.dynamic_index_in_dim(spatial_bias, group_index, 0, keepdims=False)
    blocks = v_norm.reshape(-1, BLOCK, local_width)
    mixed_cols = jnp.einsum("ts,nsc->ntc", spatial_mask, blocks, preferred_element_type=jnp.float32)
    mixed_cols = mixed_cols + block_bias[None, :, None]
    gated = (gate_u * mixed_cols.reshape(-1, local_width)).astype(jnp.bfloat16)
    out_rounded = weight_out.astype(jnp.bfloat16)
    full_out = lax.all_gather(out_rounded, "fs", axis=1, tiled=True)
    columns = full_out
    piece_scale = out_scales
    product = lax.dot_general(
        columns, gated, (((0,), (1,)), ((), ())), preferred_element_type=jnp.float32
    )
    mixer_sum = (
        lax.psum_scatter(
            (product * piece_scale[:, None]).astype(jnp.bfloat16),
            "tp",
            scatter_dimension=0,
            tiled=True,
        )
        .astype(jnp.float32)
        .T
    )
    residual = (tokens.astype(jnp.float32) + mixer_sum).astype(jnp.bfloat16)
    full_up = lax.all_gather(weight_up.astype(jnp.bfloat16), "fs", axis=0, tiled=True)
    widened_mid = residual.astype(jnp.float32)
    squares_mid = lax.psum(jnp.sum(widened_mid * widened_mid, axis=1), "tp")
    inverse_mid = lax.rsqrt(squares_mid / feature_count + 1e-06)[:, None]
    gain_piece = norm2_gain
    normed_piece = (
        lax.all_gather(residual, "tp", axis=1, tiled=True).astype(jnp.float32)
        * inverse_mid
        * gain_piece
    ).astype(jnp.bfloat16)
    pre_up = jnp.dot(normed_piece, full_up, preferred_element_type=jnp.float32)
    hidden = jnp.square(jax.nn.relu(pre_up * scale_up)).astype(jnp.bfloat16)
    down_rounded = weight_down.astype(jnp.bfloat16)
    full_down = lax.all_gather(down_rounded, "fs", axis=1, tiled=True)
    columns = full_down
    piece_scale = down_scales
    product = lax.dot_general(
        columns, hidden, (((0,), (1,)), ((), ())), preferred_element_type=jnp.float32
    )
    channel_sum = (
        lax.psum_scatter(
            (product * piece_scale[:, None]).astype(jnp.bfloat16),
            "tp",
            scatter_dimension=0,
            tiled=True,
        )
        .astype(jnp.float32)
        .T
    )
    return (residual.astype(jnp.float32) + channel_sum).astype(jnp.bfloat16)


def solution(mesh):
    placed = (
        P(("grp", "fs"), "tp"),
        P(),
        P("fs", "tp"),
        P("fs", "tp"),
        P("tp"),
        P("tp"),
        P("tp"),
        P(),
        P(),
        P("tp", "fs"),
        P("fs"),
        P(),
        P("fs", "tp"),
        P("tp"),
        P("tp", "fs"),
        P("fs"),
    )
    return jax.shard_map(
        per_device, mesh=mesh, in_specs=placed, out_specs=P(("grp", "fs"), "tp"), check_vma=False
    )
```

profile of v0, /device:TPU:0, one launch (start us, length us, event | category | flops | bytes accessed | tf_op | source)
XLA Modules:
  0.0 601.0 jit_solution(15916655100287442903)
XLA Ops:
  6.5 1.8 convert_element_type.74
  8.3 0.0 all-gather.14.cloned.1.call-update
  8.3 0.0 all-gather.10.cloned.1.call-start
  8.4 0.7 all-gather.10.cloned.1.call-update
  9.1 0.0 all-gather.12.cloned.1.call-start
  9.1 1.8 convert_element_type.73
  10.9 0.0 all-gather.12.cloned.1.call-update
  10.9 0.0 all-gather.16.cloned.1.call-start
  11.0 1.8 convert_element_type.79
  12.7 0.0 all-gather.16.cloned.1.call-update
  12.8 0.0 reduce-scatter.3.cloned.1.call-start
  12.8 1.5 fusion.8
  14.3 8.4 %psum.28 = f32[1024]{0:T(1024)S(1)} all-reduce(f32[1024]{0:T(1024)S(1)} %fusion.8), channel_id=1, replica_groups=mesh['grp'=2,'fs'=4,'tp'=4] {'tp'}, use_global_device_ids=true, to_apply=%region_1.0 | all-reduce | flops 1024 | bytes 8192 | tf_op jit(solution)/shard_map/psum | solution.py:39
  22.7 12.7 %all-gather = f32[4,1,512]{2,1,0:T(1,128)S(1)} all-gather(f32[1,1,512]{2,1,0:T(1,128)} %bitcast.33), channel_id=1, replica_groups=mesh['grp'=2,'fs'=4,'tp'=4] {'fs'}, dimensions={0}, use_global_device_ids=true | all-gather | bytes 10240 | tf_op jit(solution)/shard_map/all_gather | solution.py:31
  35.4 0.0 copy-start.4
  35.4 0.0 copy-start.5
  35.4 0.0 copy-start.8
  35.5 4.3 all-gather.14.cloned.1.call-done
  39.8 35.4 %all-gather.10.cloned.1.call-done = bf16[1024,2048]{1,0:T(8,128)(2,1)} async-done(((bf16[1024,512]{1,0:T(8,128)(2,1)}), bf16[1024,2048]{1,0:T(8,128)(2,1)}) %all-gather.10.cloned.1.call-update) | async-done | bytes 4194320 | tf_op jit(solution)/shard_map/all_gather | solution.py:43
  75.2 4.2 fusion.45
  79.4 6.0 %all-reduce = (f32[1024]{0:T(1024)S(1)}, f32[1024]{0:T(1024)S(1)}) all-reduce(f32[1024]{0:T(1024)S(1)} %get-tuple-element.6, f32[1024]{0:T(1024)S(1)} %get-tuple-element.5), channel_id=1, replica_groups=mesh['grp'=2,'fs'=4,'tp'=4] {'tp'}, use_global_device_ids=true, to_apply=%region_5.0 | all-reduce | flops 2048 | bytes 16384 | tf_op jit(solution)/shard_map/psum | solution.py:52
  85.4 0.3 multiply_convert_fusion.21
  85.8 1.1 convolution_add_fusion
  86.9 17.9 %all-gather.12.cloned.1.call-done = bf16[2048,256]{1,0:T(8,128)(2,1)} async-done(((bf16[512,256]{1,0:T(8,128)(2,1)}), bf16[2048,256]{1,0:T(8,128)(2,1)}) %all-gather.12.cloned.1.call-update) | async-done | bytes 1048592 | tf_op jit(solution)/shard_map/all_gather | solution.py:35
  104.8 28.8 %all-gather.16.cloned.1.call-done = bf16[256,2048]{1,0:T(8,128)(2,1)} async-done(((bf16[256,512]{1,0:T(8,128)(2,1)}), bf16[256,2048]{1,0:T(8,128)(2,1)}) %all-gather.16.cloned.1.call-update) | async-done | bytes 1048592 | tf_op jit(solution)/shard_map/all_gather | solution.py:69
  133.6 9.3 %fusion.6 = bf16[2048,1024]{0,1:T(8,128)(2,1)} fusion(f32[2048]{0:T(1024)S(1)} %bitcast.31, bf16[256,2048]{1,0:T(8,128)(2,1)} %all-gather.16.cloned.1.call-done, f32[1024,256]{1,0:T(8,128)S(1)} %bitcast.30, bf16[2048,256]{1,0:T(8,128)(2,1)} %all-gather.12.cloned.1.call-done, bf16[1024,2048]{1,0:T(8,128)(2,1)} %all-gather.10.cloned.1.call-done, ...), kind=kOutput, calls=%fused_computation.9 | convolution fusion | flops 2162950144 | bytes 11555840 | tf_op jit(solution)/shard_map/dot_general | solution.py:72
  142.9 0.0 reduce-scatter.3.cloned.1.call-update
  142.9 0.0 copy-start.2
  142.9 0.0 all-gather.20.cloned.1.call-start
  143.0 3.9 convert_element_type.86
  146.9 0.0 all-gather.20.cloned.1.call-update
  146.9 0.0 all-gather.22.cloned.1.call-start
  147.0 4.4 convert_element_type.88
  151.4 0.0 all-gather.22.cloned.1.call-update
  151.4 0.0 all-gather.18.cloned.1.call-start
  151.5 35.4 %reduce-scatter.3.cloned.1.call-done = bf16[512,1024]{0,1:T(8,128)(2,1)} async-done(((bf16[2048,1024]{0,1:T(8,128)(2,1)}), bf16[512,1024]{0,1:T(8,128)(2,1)}) %reduce-scatter.3.cloned.1.call-update) | async-done | bytes 1048592 | tf_op jit(solution)/shard_map/reduce_scatter | solution.py:76
  186.8 2.6 fusion.10
  189.4 0.0 all-gather.18.cloned.1.call-update
  189.5 0.0 reduce-scatter.5.cloned.1.call-start
  189.5 12.0 %all-gather.1 = f32[4,1,512]{2,1,0:T(1,128)S(1)} all-gather(f32[1,1,512]{2,1,0:T(1,128)S(1)} %bitcast.34), channel_id=1, replica_groups=mesh['grp'=2,'fs'=4,'tp'=4] {'fs'}, dimensions={0}, use_global_device_ids=true | all-gather | bytes 10240 | tf_op jit(solution)/shard_map/all_gather | solution.py:32
  201.5 6.0 %psum.31 = f32[1024]{0:T(1024)S(1)} all-reduce(f32[1024]{0:T(1024)S(1)} %get-tuple-element.9), channel_id=1, replica_groups=mesh['grp'=2,'fs'=4,'tp'=4] {'tp'}, use_global_device_ids=true, to_apply=%region_8.9 | all-reduce | flops 1024 | bytes 8192 | tf_op jit(solution)/shard_map/psum | solution.py:88
  207.6 130.4 %all-gather.20.cloned.1.call-done = bf16[2048,2048]{1,0:T(8,128)(2,1)} async-done(((bf16[512,2048]{1,0:T(8,128)(2,1)}), bf16[2048,2048]{1,0:T(8,128)(2,1)}) %all-gather.20.cloned.1.call-update) | async-done | bytes 8388624 | tf_op jit(solution)/shard_map/all_gather | solution.py:86
  337.9 149.4 %all-gather.22.cloned.1.call-done = bf16[2048,2048]{1,0:T(8,128)(2,1)} async-done(((bf16[2048,512]{1,0:T(8,128)(2,1)}), bf16[2048,2048]{1,0:T(8,128)(2,1)}) %all-gather.22.cloned.1.call-update) | async-done | bytes 8388624 | tf_op jit(solution)/shard_map/all_gather | solution.py:99
  487.3 34.2 %all-gather.18.cloned.1.call-done = bf16[1024,2048]{1,0:T(8,128)(2,1)} async-done(((bf16[1024,512]{1,0:T(8,128)(2,1)}), bf16[1024,2048]{1,0:T(8,128)(2,1)}) %all-gather.18.cloned.1.call-update) | async-done | bytes 4194320 | tf_op jit(solution)/shard_map/all_gather | solution.py:92
  521.6 25.7 %fusion.7 = bf16[2048,1024]{0,1:T(8,128)(2,1)} fusion(f32[2048]{0:T(1024)S(1)} %bitcast.32, bf16[2048,2048]{1,0:T(8,128)(2,1)} %all-gather.22.cloned.1.call-done, bf16[2048,2048]{1,0:T(8,128)(2,1)} %all-gather.20.cloned.1.call-done, bf16[1024,2048]{1,0:T(8,128)(2,1)} %all-gather.18.cloned.1.call-done, f32[2048]{0:T(1024)S(1)} %copy-done.6, ...), kind=kOutput, calls=%fused_computation.10 | convolution fusion | flops 17200840704 | bytes 25194496 | tf_op jit(solution)/shard_map/dot_general | solution.py:102
  547.3 0.0 reduce-scatter.5.cloned.1.call-update
  547.3 44.6 %reduce-scatter.5.cloned.1.call-done = bf16[512,1024]{0,1:T(8,128)(2,1)} async-done(((bf16[2048,1024]{0,1:T(8,128)(2,1)}), bf16[512,1024]{0,1:T(8,128)(2,1)}) %reduce-scatter.5.cloned.1.call-update) | async-done | bytes 1048592 | tf_op jit(solution)/shard_map/reduce_scatter | solution.py:106
  591.9 2.5 fusion.11
  (19 shorter events, 0.1 us)
Async XLA Ops:
  6.5 28.9 %copy-start = (f32[4,128]{1,0:T(4,128)S(1)}, f32[4,128]{1,0:T(4,128)}, u32[]{:S(2)}) copy-start(f32[4,128]{1,0:T(4,128)} %param.24) | copy-start | bytes 6148
  6.5 33.2 %all-gather.14.cloned.1.call-start = ((), (), s32[]{:S(2)}) async-start(), calls=%async_computation.4 | async-start | bytes 1310720 | tf_op jit(solution)/shard_map/all_gather | solution.py:36
  8.3 66.9 %all-gather.10.cloned.1.call-start = ((), (), s32[]{:S(2)}) async-start(), calls=%async_computation.2 | async-start | bytes 5242880 | tf_op jit(solution)/shard_map/all_gather | solution.py:43
  9.1 95.7 %all-gather.12.cloned.1.call-start = ((), (), s32[]{:S(2)}) async-start(), calls=%async_computation.3 | async-start | bytes 1310720 | tf_op jit(solution)/shard_map/all_gather | solution.py:35
  10.9 122.7 %all-gather.16.cloned.1.call-start = ((), (), s32[]{:S(2)}) async-start(), calls=%async_computation.5 | async-start | bytes 1310720 | tf_op jit(solution)/shard_map/all_gather | solution.py:69
  12.8 174.1 %reduce-scatter.3.cloned.1.call-start = ((), (), s32[]{:S(2)}) async-start(), calls=%async_computation.6 | async-start | bytes 5242880 | tf_op jit(solution)/shard_map/reduce_scatter | solution.py:76
  35.4 50.0 %copy-start.4 = (f32[256]{0:T(256)S(1)}, f32[256]{0:T(256)}, u32[]{:S(2)}) copy-start(f32[256]{0:T(256)} %param.22) | copy-start | bytes 3076
  35.4 98.2 %copy-start.5 = (f32[2048]{0:T(1024)S(1)}, f32[2048]{0:T(1024)}, u32[]{:S(2)}) copy-start(f32[2048]{0:T(1024)} %param.17) | copy-start | bytes 24580
  35.4 98.2 %copy-start.8 = (f32[256]{0:T(256)S(1)}, f32[256]{0:T(256)}, u32[]{:S(2)}) copy-start(f32[256]{0:T(256)} %param.20) | copy-start | bytes 3076
  142.9 43.9 %copy-start.2 = (bf16[1024,512]{1,0:T(8,128)(2,1)S(1)}, bf16[1024,512]{1,0:T(8,128)(2,1)}, u32[]{:S(2)}) copy-start(bf16[1024,512]{1,0:T(8,128)(2,1)} %param.16) | copy-start | bytes 3145732
  142.9 195.0 %all-gather.20.cloned.1.call-start = ((), (), s32[]{:S(2)}) async-start(), calls=%async_computation.8 | async-start | bytes 10485760 | tf_op jit(solution)/shard_map/all_gather | solution.py:86
  146.9 42.6 %copy-start.3 = (f32[512]{0:T(512)S(1)}, f32[512]{0:T(512)}, u32[]{:S(2)}) copy-start(f32[512]{0:T(512)} %param.31) | copy-start | bytes 6148
  146.9 374.6 %copy-start.6 = (f32[2048]{0:T(1024)S(1)}, f32[2048]{0:T(1024)}, u32[]{:S(2)}) copy-start(f32[2048]{0:T(1024)} %param.29) | copy-start | bytes 24580
  146.9 374.6 %copy-start.7 = (f32[2048]{0:T(1024)S(1)}, f32[2048]{0:T(1024)}, u32[]{:S(2)}) copy-start(f32[2048]{0:T(1024)} %param.27) | copy-start | bytes 24580
  146.9 340.4 %all-gather.22.cloned.1.call-start = ((), (), s32[]{:S(2)}) async-start(), calls=%async_computation.9 | async-start | bytes 10485760 | tf_op jit(solution)/shard_map/all_gather | solution.py:99
  151.4 370.1 %all-gather.18.cloned.1.call-start = ((), (), s32[]{:S(2)}) async-start(), calls=%async_computation.7 | async-start | bytes 5242880 | tf_op jit(solution)/shard_map/all_gather | solution.py:92
  189.5 402.4 %reduce-scatter.5.cloned.1.call-start = ((), (), s32[]{:S(2)}) async-start(), calls=%async_computation.10 | async-start | bytes 5242880 | tf_op jit(solution)/shard_map/reduce_scatter | solution.py:106
  521.6 70.3 %copy-start.1 = (bf16[1024,512]{1,0:T(8,128)(2,1)S(1)}, bf16[1024,512]{1,0:T(8,128)(2,1)}, u32[]{:S(2)}) copy-start(bf16[1024,512]{1,0:T(8,128)(2,1)} %get-tuple-element.10) | copy-start | bytes 3145732
Sparse Core Ops, SparseCore 0:
  8.9 30.8 all-gather.13
  41.3 33.8 all-gather.9
  76.8 27.9 all-gather.11
  106.2 27.3 all-gather.15
  143.1 43.7 reduce-scatter.2
  188.3 149.6 all-gather.19
  339.5 147.7 all-gather.21
  488.9 32.6 all-gather.17
  547.5 44.3 reduce-scatter.4
where the time goes:
time: 601 us
  waiting for transfers between devices  481 us (80%)
  blocking collectives  45.1 us (8%)
  matrix products  40.3 us (7%)
  other arithmetic  20.6 us (3%)
  between operations  13.3 us (2%)
    all_gather x1, waiting for transfers between devices, per_device(): full_down = lax.all_gather(down_rounded, 'fs', axis=1, tiled=True)  149 us
    all_gather x1, waiting for transfers between devices, per_device(): lax.all_gather(weight_up.astype(jnp.bfloat16), 'fs', axis=0, tiled=True)  130 us
    reduce_scatter x2, waiting for transfers between devices, per_device(): lax.psum_scatter((product * piece_scale[:, None]).astype(jnp.bfloat16), '...  79.9 us
    all_gather x1, waiting for transfers between devices, per_device(): lax.all_gather(tokens, 'tp', axis=1, tiled=True).astype(jnp.float32)  35.4 us
    all_gather x1, waiting for transfers between devices, per_device(): lax.all_gather(residual, 'tp', axis=1, tiled=True).astype(jnp.float32)  34.2 us
    all_gather x1, waiting for transfers between devices, per_device(): full_out = lax.all_gather(out_rounded, 'fs', axis=1, tiled=True)  28.8 us
    dot_general x1, matrix products, per_device(): lax.dot_general(columns, hidden, (((0,), (1,)), ((), ())), preferred_elem...  25.7 us
    all_gather x1, waiting for transfers between devices, per_device(): lax.all_gather(weight_u.astype(jnp.bfloat16), 'fs', axis=0, tiled=True)  17.9 us
  transfers between devices with their start and end apart: 9, of which 9 were waited for; matrix products, arithmetic and copies ran while one was open for 4% of the time, Pallas kernels for 0%

commit v1 on v0

--- a/solution.py
+++ b/solution.py
@@ -6,6 +6,19 @@
 GM_W = 1024
 GROUPS = 4
 BLOCK = 128
+
+
+def gather_around(shard, axis, dim):
+    ways = lax.axis_size(axis)
+    up = [(d, (d + 1) % ways) for d in range(ways)]
+    down = [(d, (d - 1) % ways) for d in range(ways)]
+    earlier, later = ([shard], [shard])
+    for _ in range(ways // 2):
+        earlier.append(lax.ppermute(earlier[-1], axis, up))
+    for _ in range((ways - 1) // 2):
+        later.append(lax.ppermute(later[-1], axis, down))
+    line = jnp.concatenate([*earlier[::-1], *later[1:]], axis=dim)
+    return jnp.roll(line, (lax.axis_index(axis) - ways // 2) * shard.shape[dim], axis=dim)
 
 
 def per_device(
@@ -89,9 +102,7 @@
     inverse_mid = lax.rsqrt(squares_mid / feature_count + 1e-06)[:, None]
     gain_piece = norm2_gain
     normed_piece = (
-        lax.all_gather(residual, "tp", axis=1, tiled=True).astype(jnp.float32)
-        * inverse_mid
-        * gain_piece
+        gather_around(residual, "tp", 1).astype(jnp.float32) * inverse_mid * gain_piece
     ).astype(jnp.bfloat16)
     pre_up = jnp.dot(normed_piece, full_up, preferred_element_type=jnp.float32)
     hidden = jnp.square(jax.nn.relu(pre_up * scale_up)).astype(jnp.bfloat16)

time: 601 us -> 566 us (0.942)
  waiting for transfers between devices: 481 us -> 426 us
  local copies, waits for them, and re-layouts: 0.05 us -> 11.5 us
  blocking collectives: 45.1 us -> 52.3 us
    all_gather x1 -> x0, waiting for transfers between devices: 34.2 us -> none  [per_device(): lax.all_gather(residual, 'tp', axis=1, tiled=True).astype(jnp.float32)]
    all_gather x1, waiting for transfers between devices: 130 us -> 96.7 us  [per_device(): lax.all_gather(weight_up.astype(jnp.bfloat16), 'fs', axis=0, tiled=True)]
    ppermute x0 -> x3, waiting for transfers between devices: none -> 14.2 us  [the longest x2 14.2 us: gather_around(): earlier.append(lax.ppermute(earlier[-1], axis, up))]
    unnamed x18 -> x25, local copies, waits for them, and re-layouts: 0.04 us -> 10.4 us
  transfers between devices with their start and end apart: 9 -> 11, of which waited for: 9 -> 9; matrix products, arithmetic and copies ran while one was open for 4% -> 6% of each run, Pallas kernels for 0% -> 0%
where the time goes in v1:
time: 566 us; the launch traced here: 565 us
  waiting for transfers between devices  426 us (75%)
  blocking collectives  52.3 us (9%)
  matrix products  40.3 us (7%)
  other arithmetic  19.7 us (3%)
  between operations  13.7 us (2%)
  local copies, waits for them, and re-layouts  11.5 us (2%)
    all_gather x1, waiting for transfers between devices, per_device(): full_down = lax.all_gather(down_rounded, 'fs', axis=1, tiled=True)  149 us
    all_gather x1, waiting for transfers between devices, per_device(): lax.all_gather(weight_up.astype(jnp.bfloat16), 'fs', axis=0, tiled=True)  96.7 us
    reduce_scatter x2, waiting for transfers between devices, per_device(): lax.psum_scatter((product * piece_scale[:, None]).astype(jnp.bfloat16), '...  78.1 us
    all_gather x1, waiting for transfers between devices, per_device(): lax.all_gather(tokens, 'tp', axis=1, tiled=True).astype(jnp.float32)  35.4 us
    all_gather x1, waiting for transfers between devices, per_device(): full_out = lax.all_gather(out_rounded, 'fs', axis=1, tiled=True)  28.8 us
    dot_general x1, matrix products, per_device(): lax.dot_general(columns, hidden, (((0,), (1,)), ((), ())), preferred_elem...  25.7 us
    all_gather x1, waiting for transfers between devices, per_device(): lax.all_gather(weight_u.astype(jnp.bfloat16), 'fs', axis=0, tiled=True)  17.9 us
    ppermute x2, waiting for transfers between devices, gather_around(): earlier.append(lax.ppermute(earlier[-1], axis, up))  14.2 us
  transfers between devices with their start and end apart: 11, of which 9 were waited for; matrix products, arithmetic and copies ran while one was open for 6% of the time, Pallas kernels for 0%

profile of v1, /device:TPU:0, one launch (start us, length us, event | category | flops | bytes accessed | tf_op | source)
XLA Modules:
  0.0 565.3 jit_solution(6685994092567540132)
XLA Ops:
  6.5 1.8 convert_element_type.74
  8.3 0.0 all-gather.9.cloned.1.call-start
  8.4 0.7 all-gather.9.cloned.1.call-update
  9.1 0.0 all-gather.11.cloned.1.call-start
  9.1 1.8 convert_element_type.73
  10.9 0.0 all-gather.11.cloned.1.call-update
  10.9 0.0 all-gather.15.cloned.1.call-start
  11.0 1.8 convert_element_type.79
  12.7 0.0 all-gather.15.cloned.1.call-update
  12.8 0.0 reduce-scatter.3.cloned.1.call-start
  12.8 1.5 fusion.10
  14.4 8.4 %psum.28 = f32[1024]{0:T(1024)S(1)} all-reduce(f32[1024]{0:T(1024)S(1)} %fusion.10), channel_id=1, replica_groups=mesh['grp'=2,'fs'=4,'tp'=4] {'tp'}, use_global_device_ids=true, to_apply=%region_1.0 | all-reduce | flops 1024 | bytes 8192 | tf_op jit(solution)/shard_map/psum | solution.py:52
  22.7 12.7 %all-gather = f32[4,1,512]{2,1,0:T(1,128)S(1)} all-gather(f32[1,1,512]{2,1,0:T(1,128)} %bitcast.33), channel_id=1, replica_groups=mesh['grp'=2,'fs'=4,'tp'=4] {'fs'}, dimensions={0}, use_global_device_ids=true | all-gather | bytes 10240 | tf_op jit(solution)/shard_map/all_gather | solution.py:44
  35.5 4.3 all-gather.13.cloned.1.call-done
  39.8 35.4 %all-gather.9.cloned.1.call-done = bf16[1024,2048]{1,0:T(8,128)(2,1)} async-done(((bf16[1024,512]{1,0:T(8,128)(2,1)}), bf16[1024,2048]{1,0:T(8,128)(2,1)}) %all-gather.9.cloned.1.call-update) | async-done | bytes 4194320 | tf_op jit(solution)/shard_map/all_gather | solution.py:56
  75.2 4.2 fusion.50
  79.4 6.0 %all-reduce = (f32[1024]{0:T(1024)S(1)}, f32[1024]{0:T(1024)S(1)}) all-reduce(f32[1024]{0:T(1024)S(1)} %get-tuple-element.6, f32[1024]{0:T(1024)S(1)} %get-tuple-element.5), channel_id=1, replica_groups=mesh['grp'=2,'fs'=4,'tp'=4] {'tp'}, use_global_device_ids=true, to_apply=%region_5.0 | all-reduce | flops 2048 | bytes 16384 | tf_op jit(solution)/shard_map/psum | solution.py:65
  85.4 0.3 multiply_convert_fusion.21
  85.8 1.1 convolution_add_fusion
  86.9 17.9 %all-gather.11.cloned.1.call-done = bf16[2048,256]{1,0:T(8,128)(2,1)} async-done(((bf16[512,256]{1,0:T(8,128)(2,1)}), bf16[2048,256]{1,0:T(8,128)(2,1)}) %all-gather.11.cloned.1.call-update) | async-done | bytes 1048592 | tf_op jit(solution)/shard_map/all_gather | solution.py:48
  104.8 28.8 %all-gather.15.cloned.1.call-done = bf16[256,2048]{1,0:T(8,128)(2,1)} async-done(((bf16[256,512]{1,0:T(8,128)(2,1)}), bf16[256,2048]{1,0:T(8,128)(2,1)}) %all-gather.15.cloned.1.call-update) | async-done | bytes 1048592 | tf_op jit(solution)/shard_map/all_gather | solution.py:82
  133.6 9.3 %fusion.8 = bf16[2048,1024]{0,1:T(8,128)(2,1)} fusion(f32[2048]{0:T(1024)S(1)} %bitcast.31, bf16[256,2048]{1,0:T(8,128)(2,1)} %all-gather.15.cloned.1.call-done, f32[1024,256]{1,0:T(8,128)S(1)} %bitcast.30, bf16[2048,256]{1,0:T(8,128)(2,1)} %all-gather.11.cloned.1.call-done, bf16[1024,2048]{1,0:T(8,128)(2,1)} %all-gather.9.cloned.1.call-done, ...), kind=kOutput, calls=%fused_computation.10 | convolution fusion | flops 2162950144 | bytes 11555840 | tf_op jit(solution)/shard_map/dot_general | solution.py:85
  142.9 0.0 reduce-scatter.3.cloned.1.call-update
  142.9 0.0 all-gather.17.cloned.1.call-start
  143.0 3.9 convert_element_type.86
  147.0 0.0 all-gather.19.cloned.1.call-start
  147.0 4.4 convert_element_type.88
  151.4 0.0 reduce-scatter.5.cloned.1.call-start
  151.5 35.4 %reduce-scatter.3.cloned.1.call-done = bf16[512,1024]{0,1:T(8,128)(2,1)} async-done(((bf16[2048,1024]{0,1:T(8,128)(2,1)}), bf16[512,1024]{0,1:T(8,128)(2,1)}) %reduce-scatter.3.cloned.1.call-update) | async-done | bytes 1048592 | tf_op jit(solution)/shard_map/reduce_scatter | solution.py:89
  186.8 1.7 fusion.12
  188.6 0.1 collective-permute-start
  188.6 14.2 %collective-permute-done = bf16[1024,512]{1,0:T(8,128)(2,1)S(1)} collective-permute-done((bf16[1024,512]{1,0:T(8,128)(2,1)S(1)}, bf16[1024,512]{1,0:T(8,128)(2,1)S(1)}, u32[]{:S(2)}, u32[]{:S(2)}) %collective-permute-start) | collective-permute-done | bytes 1048608 | tf_op jit(solution)/shard_map/ppermute | solution.py:17
  202.8 1.7 collective-permute-start.2
  204.6 14.1 %all-gather.1 = f32[4,1,512]{2,1,0:T(1,128)S(1)} all-gather(f32[1,1,512]{2,1,0:T(1,128)S(1)} %bitcast.34), channel_id=1, replica_groups=mesh['grp'=2,'fs'=4,'tp'=4] {'fs'}, dimensions={0}, use_global_device_ids=true | all-gather | bytes 10240 | tf_op jit(solution)/shard_map/all_gather | solution.py:45
  218.7 11.2 %psum.31 = f32[1024]{0:T(1024)S(1)} all-reduce(f32[1024]{0:T(1024)S(1)} %get-tuple-element.9), channel_id=1, replica_groups=mesh['grp'=2,'fs'=4,'tp'=4] {'tp'}, use_global_device_ids=true, to_apply=%region_8.9 | all-reduce | flops 1024 | bytes 8192 | tf_op jit(solution)/shard_map/psum | solution.py:101
  229.9 2.3 constant_dynamic-update-slice_fusion.7
  232.2 1.1 constant_dynamic-update-slice_fusion.6
  233.3 1.1 constant_dynamic-update-slice_fusion.5
  234.4 1.1 constant_dynamic-update-slice_fusion.4
  235.6 2.3 constant_dynamic-update-slice_fusion.3
  237.9 1.1 constant_dynamic-update-slice_fusion.2
  239.1 1.1 constant_dynamic-update-slice_fusion.1
  240.2 1.1 constant_dynamic-update-slice_fusion
  241.3 96.7 %all-gather.17.cloned.1.call-done = bf16[2048,2048]{1,0:T(8,128)(2,1)} async-done(((bf16[512,2048]{1,0:T(8,128)(2,1)}), bf16[2048,2048]{1,0:T(8,128)(2,1)}) %all-gather.17.cloned.1.call-update) | async-done | bytes 8388624 | tf_op jit(solution)/shard_map/all_gather | solution.py:99
  338.1 149.4 %all-gather.19.cloned.1.call-done = bf16[2048,2048]{1,0:T(8,128)(2,1)} async-done(((bf16[2048,512]{1,0:T(8,128)(2,1)}), bf16[2048,2048]{1,0:T(8,128)(2,1)}) %all-gather.19.cloned.1.call-update) | async-done | bytes 8388624 | tf_op jit(solution)/shard_map/all_gather | solution.py:110
  487.5 25.7 %fusion.9 = bf16[2048,1024]{0,1:T(8,128)(2,1)} fusion(f32[2048]{0:T(1024)S(1)} %bitcast.32, bf16[2048,2048]{1,0:T(8,128)(2,1)} %all-gather.19.cloned.1.call-done, bf16[2048,2048]{1,0:T(8,128)(2,1)} %all-gather.17.cloned.1.call-done, f32[2048]{0:T(1024)S(1)} %copy-done.6, f32[2048]{0:T(1024)S(1)} %copy-done.7, f32[1024]{0:T(1024)S(1)} %add_rsqrt_fusion, ...), kind=kOutput, calls=%fused_computation.11 | convolution fusion | flops 17200840704 | bytes 25194500 | tf_op jit(solution)/shard_map/dot_general | solution.py:113
  513.1 42.7 %reduce-scatter.5.cloned.1.call-done = bf16[512,1024]{0,1:T(8,128)(2,1)} async-done(((bf16[2048,1024]{0,1:T(8,128)(2,1)}), bf16[512,1024]{0,1:T(8,128)(2,1)}) %reduce-scatter.5.cloned.1.call-update) | async-done | bytes 1048592 | tf_op jit(solution)/shard_map/reduce_scatter | solution.py:117
  555.9 2.5 fusion.13
  (30 shorter events, 0.1 us)
Async XLA Ops:
  6.5 28.9 %copy-start = (f32[4,128]{1,0:T(4,128)S(1)}, f32[4,128]{1,0:T(4,128)}, u32[]{:S(2)}) copy-start(f32[4,128]{1,0:T(4,128)} %param.24) | copy-start | bytes 6148
  6.5 33.2 %all-gather.13.cloned.1.call-start = ((), (), s32[]{:S(2)}) async-start(), calls=%async_computation.4 | async-start | bytes 1310720 | tf_op jit(solution)/shard_map/all_gather | solution.py:49
  8.3 66.9 %all-gather.9.cloned.1.call-start = ((), (), s32[]{:S(2)}) async-start(), calls=%async_computation.2 | async-start | bytes 5242880 | tf_op jit(solution)/shard_map/all_gather | solution.py:56
  9.1 95.7 %all-gather.11.cloned.1.call-start = ((), (), s32[]{:S(2)}) async-start(), calls=%async_computation.3 | async-start | bytes 1310720 | tf_op jit(solution)/shard_map/all_gather | solution.py:48
  10.9 122.7 %all-gather.15.cloned.1.call-start = ((), (), s32[]{:S(2)}) async-start(), calls=%async_computation.5 | async-start | bytes 1310720 | tf_op jit(solution)/shard_map/all_gather | solution.py:82
  12.8 174.1 %reduce-scatter.3.cloned.1.call-start = ((), (), s32[]{:S(2)}) async-start(), calls=%async_computation.6 | async-start | bytes 5242880 | tf_op jit(solution)/shard_map/reduce_scatter | solution.py:89
  35.4 50.0 %copy-start.4 = (f32[256]{0:T(256)S(1)}, f32[256]{0:T(256)}, u32[]{:S(2)}) copy-start(f32[256]{0:T(256)} %param.22) | copy-start | bytes 3076
  35.4 98.2 %copy-start.5 = (f32[2048]{0:T(1024)S(1)}, f32[2048]{0:T(1024)}, u32[]{:S(2)}) copy-start(f32[2048]{0:T(1024)} %param.17) | copy-start | bytes 24580
  35.4 98.2 %copy-start.8 = (f32[256]{0:T(256)S(1)}, f32[256]{0:T(256)}, u32[]{:S(2)}) copy-start(f32[256]{0:T(256)} %param.20) | copy-start | bytes 3076
  142.9 43.9 %copy-start.2 = (bf16[1024,512]{1,0:T(8,128)(2,1)S(1)}, bf16[1024,512]{1,0:T(8,128)(2,1)}, u32[]{:S(2)}) copy-start(bf16[1024,512]{1,0:T(8,128)(2,1)} %param.16) | copy-start | bytes 3145732
  142.9 195.1 %all-gather.17.cloned.1.call-start = ((), (), s32[]{:S(2)}) async-start(), calls=%async_computation.7 | async-start | bytes 10485760 | tf_op jit(solution)/shard_map/all_gather | solution.py:99
  146.9 57.6 %copy-start.3 = (f32[512]{0:T(512)S(1)}, f32[512]{0:T(512)}, u32[]{:S(2)}) copy-start(f32[512]{0:T(512)} %param.31) | copy-start | bytes 6148
  147.0 340.5 %all-gather.19.cloned.1.call-start = ((), (), s32[]{:S(2)}) async-start(), calls=%async_computation.8 | async-start | bytes 10485760 | tf_op jit(solution)/shard_map/all_gather | solution.py:110
  151.4 404.5 %reduce-scatter.5.cloned.1.call-start = ((), (), s32[]{:S(2)}) async-start(), calls=%async_computation.9 | async-start | bytes 5242880 | tf_op jit(solution)/shard_map/reduce_scatter | solution.py:117
  188.6 14.3 %collective-permute-start = (bf16[1024,512]{1,0:T(8,128)(2,1)S(1)}, bf16[1024,512]{1,0:T(8,128)(2,1)S(1)}, u32[]{:S(2)}, u32[]{:S(2)}) collective-permute-start(bf16[1024,512]{1,0:T(8,128)(2,1)S(1)} %get-tuple-element.10), channel_id=1, source_target_pairs={{0,1},{1,2},{2,3},{3,0},{4,5},{5,6},{6,7},{7,4},{8,9},{9,10},{10,1... | collective-permute-start | bytes 3145736 | tf_op jit(solution)/shard_map/ppermute | solution.py:17
  202.8 27.1 %collective-permute-start.1 = (bf16[1024,512]{1,0:T(8,128)(2,1)S(1)}, bf16[1024,512]{1,0:T(8,128)(2,1)}, u32[]{:S(2)}, u32[]{:S(2)}) collective-permute-start(bf16[1024,512]{1,0:T(8,128)(2,1)S(1)} %collective-permute-done), channel_id=1, source_target_pairs={{0,1},{1,2},{2,3},{3,0},{4,5},{5,6},{6,7},{7,4},{8,9},{9,10},{10,1... | collective-permute-start | bytes 3145736 | tf_op jit(solution)/shard_map/ppermute | solution.py:17
  202.8 31.6 %collective-permute-start.2 = (bf16[1024,512]{1,0:T(8,128)(2,1)S(1)}, bf16[1024,512]{1,0:T(8,128)(2,1)S(1)}, u32[]{:S(2)}, u32[]{:S(2)}) collective-permute-start(bf16[1024,512]{1,0:T(8,128)(2,1)S(1)} %get-tuple-element.10), channel_id=1, source_target_pairs={{0,3},{1,0},{2,1},{3,2},{4,7},{5,4},{6,5},{7,6},{8,11},{9,8},{10,9... | collective-permute-start | bytes 3145736 | tf_op jit(solution)/shard_map/ppermute | solution.py:19
  229.9 257.6 %copy-start.6 = (f32[2048]{0:T(1024)S(1)}, f32[2048]{0:T(1024)}, u32[]{:S(2)}) copy-start(f32[2048]{0:T(1024)} %param.29) | copy-start | bytes 24580
  229.9 257.6 %copy-start.7 = (f32[2048]{0:T(1024)S(1)}, f32[2048]{0:T(1024)}, u32[]{:S(2)}) copy-start(f32[2048]{0:T(1024)} %param.27) | copy-start | bytes 24580
  487.5 71.0 %copy-start.1 = (f32[4,128]{1,0:T(4,128)S(1)}, f32[4,128]{1,0:T(4,128)}, u32[]{:S(2)}) copy-start(f32[4,128]{1,0:T(4,128)} %param.24) | copy-start | bytes 6148
Sparse Core Ops, SparseCore 0:
  8.9 30.8 all-gather.12
  41.3 33.8 all-gather.8
  76.8 27.9 all-gather.10
  106.2 27.3 all-gather.14
  143.1 43.7 reduce-scatter.2
  188.3 149.7 all-gather.16
  339.6 147.7 all-gather.18
  513.3 42.5 reduce-scatter.4
